TPU v7x, 512 devices: a whole 4x4x16 slice. The times are simulated.
512 devices in a mesh: kv: 16 (over y, x), tp: 32 (over z, core).
Axes of the slice: x: 4, y: 4, z: 16, core: 2. Of those that a mesh axis runs over, the one named last changes fastest.
Arguments:
- residual: bfloat16 [512, 2048], P('tp', 'kv'), may hold values from -64 to 64
- prior_state: float32 [512, 16, 128, 128], P('tp', 'kv'), may hold values from -6 to 6
- w_query: bfloat16 [2048, 2048], P('tp', 'kv'), may hold values from -0.125 to 0.125
- w_forget: bfloat16 [2048, 2048], P('tp', 'kv'), may hold values from -0.125 to 0.125
- w_value: bfloat16 [2048, 2048], P('tp', 'kv'), may hold values from -0.125 to 0.125
- w_outgate: bfloat16 [2048, 2048], P('tp', 'kv'), may hold values from -0.125 to 0.125
- forget_floor: float32 [2048], P('kv'), may hold values from 0.05 to 0.9
- group_gain: float32 [2048], P('kv'), may hold values from 0.1 to 1.9
- w_mix_out: bfloat16 [2048, 2048], P('kv', 'tp'), may hold values from -0.397747564 to 0.397747564
- gain_mix_pre: float32 [2048], replicated, may hold values from 0.1 to 1.9
- gain_mix_post: float32 [2048], replicated, may hold values from 0.05 to 1.9
- gain_mlp_pre: float32 [2048], replicated, may hold values from 0.1 to 1.9
- gain_mlp_post: float32 [2048], replicated, may hold values from 0.1 to 1.9
- w_up: bfloat16 [2048, 8192], P('tp', 'kv'), may hold values from -0.125 to 0.125
- w_down: bfloat16 [8192, 2048], P('kv', 'tp'), may hold values from -0.198873782 to 0.198873782
Outputs:
- layer_out: bfloat16 [512, 2048], P('tp', 'kv')
- new_state: float32 [512, 16, 128, 128], P('tp', 'kv')
All inputs are finite; a program needn't handle non-finite values.
Results may differ from a plain program's by a relative error of at most 0.015.
Values may be sent and summed in bfloat16 or wider, within the bound.
No kernel may reach another device: no remote copies, remote signals or barrier semaphores. Data moves between devices by JAX's collectives and lax.ppermute only.
A program may use at most 64 MiB of HBM per device.

v0:
```python
import jax
import jax.numpy as jnp
from jax import lax
from jax.sharding import PartitionSpec as P

HEAD_DIM = 128
epsilon = 1e-06


def side_by_side(arrays, axis, dim, along):
    widths = [a.shape[along] for a in arrays]
    both = jnp.concatenate(arrays, axis=along)
    filled = lax.all_gather(both, axis, axis=dim, tiled=True)
    return tuple(jnp.split(filled, [sum(widths[:k]) for k in range(1, len(widths))], axis=along))


def split_up(value, dim, devices):
    before, after = (value.shape[:dim], value.shape[dim + 1 :])
    return jnp.moveaxis(value.reshape(*before, devices, -1, *after), dim, 0)


def summed_on_arrival(value, axis, dim):
    devices = lax.axis_size(axis)
    blocks = lax.all_to_all(split_up(value, dim, devices), axis, 0, 0, tiled=True)
    return jnp.sum(blocks, axis=0)


def from_everyone(value, axis):
    devices = lax.axis_size(axis)
    return lax.all_to_all(
        jnp.broadcast_to(value[None], (devices, *value.shape)), axis, 0, 0, tiled=True
    )


def taken_together(value, axis):
    return from_everyone(value, axis).sum(axis=0)


def inverse_norm(values):
    return lax.rsqrt(jnp.mean(values * values, axis=-1, keepdims=True) + epsilon)


def shards(
    residual,
    prior_state,
    w_query,
    w_forget,
    w_value,
    w_outgate,
    forget_floor,
    group_gain,
    w_mix_out,
    gain_mix_pre,
    gain_mix_post,
    gain_mlp_pre,
    gain_mlp_post,
    w_up,
    w_down,
):
    batch_rows = residual.shape[0]
    own_cols = residual.shape[1]
    offset = lax.axis_index("kv") * own_cols
    whole_rows = lax.all_gather(residual, "kv", axis=1, tiled=True)
    full_width = whole_rows.shape[1]
    stream = whole_rows.astype(jnp.float32)
    normed = (stream * inverse_norm(stream) * gain_mix_pre).astype(jnp.bfloat16)
    pieces = side_by_side((w_query, w_forget, w_value, w_outgate), "tp", 0, 1)
    left_part = normed
    totals = tuple(
        (
            jnp.dot(left_part, weight_part, preferred_element_type=jnp.float32)
            for weight_part in pieces
        )
    )
    query_pre, forget_pre, value_pre, gate_pre = (
        running.astype(jnp.bfloat16) for running in totals
    )
    heads_here = prior_state.shape[1]
    head_shape = (batch_rows, heads_here, HEAD_DIM)
    query_act = jax.nn.silu(query_pre.astype(jnp.float32)).reshape(head_shape)
    lower_bound = forget_floor.reshape(heads_here, HEAD_DIM)
    forget = lower_bound + (1.0 - lower_bound) * jax.nn.sigmoid(
        forget_pre.astype(jnp.float32).reshape(head_shape)
    )
    values_in = value_pre.astype(jnp.float32).reshape(head_shape)
    new_state = (
        forget[..., None] * prior_state + (1.0 - forget)[..., None] * values_in[:, :, None, :]
    )
    readout = jnp.einsum("bhk,bhkv->bhv", query_act, new_state, precision=lax.Precision.HIGHEST)
    gate_act = jax.nn.sigmoid(gate_pre.astype(jnp.float32).reshape(head_shape))
    gated_out = (
        readout * inverse_norm(readout) * group_gain.reshape(heads_here, HEAD_DIM) * gate_act
    ).astype(jnp.bfloat16)
    gated_flat = gated_out.reshape(batch_rows, heads_here * HEAD_DIM)
    mixed_part = jnp.dot(
        gated_flat,
        lax.all_gather(w_mix_out, "tp", axis=1, tiled=True),
        preferred_element_type=jnp.float32,
    )
    mixed_sum = summed_on_arrival(mixed_part, "kv", 1)
    mix_total = taken_together(jnp.sum(mixed_sum * mixed_sum, axis=1), "kv")
    mix_scale = lax.rsqrt(mix_total / full_width + epsilon)[:, None]
    post_gain = lax.dynamic_slice_in_dim(gain_mix_post, offset, own_cols, 0)
    after_mix = (residual.astype(jnp.float32) + mixed_sum * mix_scale * post_gain).astype(
        jnp.bfloat16
    )
    after_wide = after_mix.astype(jnp.float32)
    stream_total = lax.psum(jnp.sum(after_wide * after_wide, axis=1), "kv")
    stream_scale = lax.rsqrt(stream_total / full_width + epsilon)[:, None]
    pre_gain = lax.dynamic_slice_in_dim(gain_mlp_pre, offset, own_cols, 0)
    hidden_own = (after_wide * stream_scale * pre_gain).astype(jnp.bfloat16)
    hidden_in = lax.all_gather(hidden_own, "kv", axis=1, tiled=True)
    left_part = hidden_in
    up_sum = jnp.dot(
        left_part,
        lax.all_gather(w_up, "tp", axis=0, tiled=True),
        preferred_element_type=jnp.float32,
    )
    squared = jnp.square(jax.nn.relu(up_sum)).astype(jnp.bfloat16)
    channel_part = jnp.dot(
        squared,
        lax.all_gather(w_down, "tp", axis=1, tiled=True),
        preferred_element_type=jnp.float32,
    )
    out_gain = lax.dynamic_slice_in_dim(gain_mlp_post, offset, own_cols, 0)
    own_part = summed_on_arrival(channel_part, "kv", 1)
    layer_out = (after_mix.astype(jnp.float32) + own_part * out_gain).astype(jnp.bfloat16)
    return (layer_out, new_state)


def solution(mesh):
    return jax.shard_map(
        shards,
        mesh=mesh,
        in_specs=(
            P("tp", "kv"),
            P("tp", "kv", None, None),
            P("tp", "kv"),
            P("tp", "kv"),
            P("tp", "kv"),
            P("tp", "kv"),
            P("kv"),
            P("kv"),
            P("kv", "tp"),
            P(),
            P(),
            P(),
            P(),
            P("tp", "kv"),
            P("kv", "tp"),
        ),
        out_specs=(P("tp", "kv"), P("tp", "kv", None, None)),
        check_vma=False,
    )
```

profile of v0, /device:TPU:1, one launch (start us, length us, event | category | flops | bytes accessed | tf_op | source)
XLA Modules:
  0.0 254.0 jit_solution(2061126913411901489)
XLA Ops:
  7.2 1.5 pad_maximum_fusion
  8.8 0.7 all-gather.6.cloned.1.call-update
  9.6 0.7 all-gather.8.cloned.1.call-update
  10.2 19.4 %all_gather.18 = bf16[16,2048]{1,0:T(8,128)(2,1)S(1)} all-gather(bf16[16,128]{1,0:T(8,128)(2,1)} %param.15), channel_id=1, replica_groups=mesh['kv'=16,'tp'=32] {'kv'}, dimensions={1}, use_global_device_ids=true | all-gather | bytes 69632 | tf_op jit(solution)/shard_map/all_gather | solution.py:63
  29.8 0.7 broadcast_subtract_fusion.1
  30.5 44.0 %all_gather.20 = bf16[128,2048]{0,1:T(8,128)(2,1)S(1)} all-gather(bf16[128,64]{0,1:T(8,128)(2,1)} %param.23), channel_id=1, replica_groups=mesh['kv'=16,'tp'=32] {'tp'}, dimensions={1}, use_global_device_ids=true | all-gather | bytes 540672 | tf_op jit(solution)/shard_map/all_gather | solution.py:97
  74.5 13.5 %all-gather.4.cloned.1.call-done = bf16[2048,512]{1,0:T(8,128)(2,1)} async-done(((bf16[64,512]{1,0:T(8,128)(2,1)}), bf16[2048,512]{1,0:T(8,128)(2,1)}) %all-gather.4.cloned.1.call-update) | async-done | bytes 2097168 | tf_op jit(solution)/shard_map/all_gather | solution.py:13
  87.9 1.3 fusion.9
  89.2 1.3 divide_multiply_fusion
  90.6 1.3 broadcast_subtract_fusion
  92.5 1.0 fusion.19
  93.6 1.5 convolution_bitcast_fusion
  95.1 13.2 %all_to_all.16 = f32[16,16,128]{2,1,0:T(8,128)S(1)} all-to-all(f32[16,16,128]{2,1,0:T(8,128)S(1)} %convolution_bitcast_fusion), channel_id=1, replica_groups=mesh['kv'=16,'tp'=32] {'kv'}, dimensions={0} | all-to-all | bytes 262144 | tf_op jit(solution)/shard_map/all_to_all | solution.py:24
  109.1 3.4 %all-to-all-start.1 = ((f32[16,1,16]{2,1,0:T(1,128)}), f32[16,1,16]{2,1,0:T(1,128)S(1)}, u32[]{:S(2)}, u32[]{:S(2)}) async-start(f32[16,1,16]{2,1,0:T(1,128)} %broadcast_in_dim.2), calls=%async_computation.1 | async-start | bytes 16384 | tf_op jit(solution)/shard_map/all_to_all | solution.py:30
  112.6 0.8 dynamic_slice.9
  113.3 0.8 dynamic_slice.10
  114.1 4.7 %all-to-all-done.1 = f32[16,1,16]{2,1,0:T(1,128)S(1)} async-done(((f32[16,1,16]{2,1,0:T(1,128)}), f32[16,1,16]{2,1,0:T(1,128)S(1)}, u32[]{:S(2)}, u32[]{:S(2)}) %all-to-all-start.1) | async-done | bytes 1056 | tf_op jit(solution)/shard_map/all_to_all | solution.py:30
  119.0 30.4 %psum.7 = f32[16]{0:T(128)S(1)} all-reduce(f32[16]{0:T(128)S(1)} %get-tuple-element.2), channel_id=1, replica_groups=mesh['kv'=16,'tp'=32] {'kv'}, use_global_device_ids=true, to_apply=%region_6.7 | all-reduce | flops 16 | bytes 128 | tf_op jit(solution)/shard_map/psum | solution.py:108
  149.5 16.5 %all_gather.21 = bf16[16,2048]{1,0:T(8,128)(2,1)S(1)} all-gather(bf16[16,128]{1,0:T(8,128)(2,1)S(1)} %fusion.32), channel_id=1, replica_groups=mesh['kv'=16,'tp'=32] {'kv'}, dimensions={1}, use_global_device_ids=true | all-gather | bytes 69632 | tf_op jit(solution)/shard_map/all_gather | solution.py:112
  166.0 63.7 %all-gather.8.cloned.1.call-done = bf16[512,2048]{0,1:T(8,128)(2,1)} async-done(((bf16[512,64]{0,1:T(8,128)(2,1)}), bf16[512,2048]{0,1:T(8,128)(2,1)}) %all-gather.8.cloned.1.call-update) | async-done | bytes 2097168 | tf_op jit(solution)/shard_map/all_gather | solution.py:122
  229.7 3.2 %convolution_bitcast_fusion.1 = f32[2,16,8,128]{3,2,1,0:T(8,128)S(1)} fusion(bf16[512,2048]{0,1:T(8,128)(2,1)} %all-gather.8.cloned.1.call-done, bf16[16,2048]{1,0:T(8,128)(2,1)S(1)} %all_gather.21, bf16[2048,512]{1,0:T(8,128)(2,1)} %all-gather.6.cloned.1.call-done), kind=kOutput, calls=%fused_computation.1 | convolution fusion | flops 67133440 | bytes 4390912 | tf_op jit(solution)/shard_map/dot_general | solution.py:120
  233.5 6.5 %all-to-all-start.2 = ((f32[16,16,128]{2,1,0:T(8,128)}), f32[16,16,128]{2,1,0:T(8,128)S(1)}, u32[]{:S(2)}, u32[]{:S(2)}) async-start(f32[16,16,128]{2,1,0:T(8,128)} %bitcast.30), calls=%async_computation.2 | async-start | bytes 262144 | tf_op jit(solution)/shard_map/all_to_all | solution.py:24
  240.1 0.8 dynamic_slice.11
  240.8 6.1 %all-to-all-done.2 = f32[16,16,128]{2,1,0:T(8,128)S(1)} async-done(((f32[16,16,128]{2,1,0:T(8,128)}), f32[16,16,128]{2,1,0:T(8,128)S(1)}, u32[]{:S(2)}, u32[]{:S(2)}) %all-to-all-start.2) | async-done | bytes 131104 | tf_op jit(solution)/shard_map/all_to_all | solution.py:24
  (33 shorter events, 3.4 us)
Async XLA Ops:
  7.2 83.4 %copy-start.5 = (f32[128]{0:T(128)S(1)}, f32[128]{0:T(128)}, u32[]{:S(2)}) copy-start(f32[128]{0:T(128)} %param.21) | copy-start | bytes 1540
  7.2 83.4 %copy-start.3 = (f32[2048]{0:T(1024)S(1)}, f32[2048]{0:T(1024)}, u32[]{:S(2)}) copy-start(f32[2048]{0:T(1024)} %param.24) | copy-start | bytes 24580
  7.2 84.7 %copy-start.1 = (f32[16,1,128,128]{3,2,1,0:T(8,128)S(1)}, f32[16,1,128,128]{3,2,1,0:T(8,128)}, u32[]{:S(2)}) copy-start(f32[16,1,128,128]{3,2,1,0:T(8,128)} %param.16) | copy-start | bytes 3145732
  7.2 80.7 %all-gather.4.cloned.1.call-start = ((), (), s32[]{:S(2)}) async-start(), calls=%async_computation.3 | async-start | bytes 2162688 | tf_op jit(solution)/shard_map/all_gather | solution.py:13
  8.8 157.2 %all-gather.6.cloned.1.call-start = ((), (), s32[]{:S(2)}) async-start(), calls=%async_computation.4 | async-start | bytes 2162688 | tf_op jit(solution)/shard_map/all_gather | solution.py:116
  9.5 220.2 %all-gather.8.cloned.1.call-start = ((), (), s32[]{:S(2)}) async-start(), calls=%async_computation.5 | async-start | bytes 2162688 | tf_op jit(solution)/shard_map/all_gather | solution.py:122
  90.6 3.1 %copy-start.4 = (f32[128]{0:T(128)S(1)}, f32[128]{0:T(128)}, u32[]{:S(2)}) copy-start(f32[128]{0:T(128)} %param.22) | copy-start | bytes 1540
  91.9 26.9 %copy-start.2 = (bf16[16,128]{1,0:T(8,128)(2,1)S(1)}, bf16[16,128]{1,0:T(8,128)(2,1)}, u32[]{:S(2)}) copy-start(bf16[16,128]{1,0:T(8,128)(2,1)} %param.15) | copy-start | bytes 12292
  92.5 140.3 %copy-start = (f32[16,1,128,128]{3,2,1,0:T(8,128)}, f32[16,1,128,128]{3,2,1,0:T(8,128)S(1)}, u32[]{:S(2)}) copy-start(f32[16,1,128,128]{3,2,1,0:T(8,128)S(1)} %multiply_add_fusion) | copy-start | bytes 3145732
  109.1 9.7 %all-to-all-start.1 = ((f32[16,1,16]{2,1,0:T(1,128)}), f32[16,1,16]{2,1,0:T(1,128)S(1)}, u32[]{:S(2)}, u32[]{:S(2)}) async-start(f32[16,1,16]{2,1,0:T(1,128)} %broadcast_in_dim.2), calls=%async_computation.1 | async-start | bytes 16384 | tf_op jit(solution)/shard_map/all_to_all | solution.py:30
  233.5 13.4 %all-to-all-start.2 = ((f32[16,16,128]{2,1,0:T(8,128)}), f32[16,16,128]{2,1,0:T(8,128)S(1)}, u32[]{:S(2)}, u32[]{:S(2)}) async-start(f32[16,16,128]{2,1,0:T(8,128)} %bitcast.30), calls=%async_computation.2 | async-start | bytes 262144 | tf_op jit(solution)/shard_map/all_to_all | solution.py:24
Sparse Core Ops, SparseCore 0:
  10.7 77.1 all-gather.3
  90.1 68.8 all-gather.5
  161.1 68.5 all-gather.7
where the time goes:
time: 255 us; the launch traced here: 254 us
  blocking collectives  124 us (49%)
  waiting for transfers between devices  89.3 us (35%)
  between operations  13.9 us (5%)
  starting transfers between devices  10.1 us (4%)
  matrix products  9.56 us (4%)
  other arithmetic  4.07 us (2%)
  local copies, waits for them, and re-layouts  3.6 us (1%)
    all_gather x1, waiting for transfers between devices, shards(): lax.all_gather(w_down, 'tp', axis=1, tiled=True)  63.7 us
    all_gather x1, blocking collectives, shards(): lax.all_gather(w_mix_out, 'tp', axis=1, tiled=True)  44 us
    psum x1, blocking collectives, shards(): stream_total = lax.psum(jnp.sum(after_wide * after_wide, axis=1), 'kv')  30.4 us
    all_gather x1, blocking collectives, shards(): whole_rows = lax.all_gather(residual, 'kv', axis=1, tiled=True)  19.4 us
    all_gather x1, blocking collectives, shards(): hidden_in = lax.all_gather(hidden_own, 'kv', axis=1, tiled=True)  16.5 us
    all_gather x1, waiting for transfers between devices, side_by_side(): filled = lax.all_gather(both, axis, axis=dim, tiled=True)  13.5 us
    all_to_all x1, blocking collectives, summed_on_arrival(): lax.all_to_all(split_up(value, dim, devices), axis, 0, 0, tiled=True)  13.2 us
    all_to_all x1, starting transfers between devices, summed_on_arrival(): lax.all_to_all(split_up(value, dim, devices), axis, 0, 0, tiled=True)  6.53 us
  transfers between devices with their start and end apart: 5, of which 4 were waited for; matrix products, arithmetic and copies ran while one was open for 4% of the time, Pallas kernels for 0%

commit v1 on v0

--- a/solution.py
+++ b/solution.py
@@ -60,7 +60,12 @@
     batch_rows = residual.shape[0]
     own_cols = residual.shape[1]
     offset = lax.axis_index("kv") * own_cols
-    whole_rows = lax.all_gather(residual, "kv", axis=1, tiled=True)
+    ring = [residual]
+    for hop in range(15):
+        ring.append(lax.ppermute(ring[-1], "kv", [(dev, (dev + 1) % 16) for dev in range(16)]))
+    whole_rows = jnp.roll(
+        jnp.concatenate(ring[::-1], axis=1), (lax.axis_index("kv") + 1) * ring[0].shape[1], axis=1
+    )
     full_width = whole_rows.shape[1]
     stream = whole_rows.astype(jnp.float32)
     normed = (stream * inverse_norm(stream) * gain_mix_pre).astype(jnp.bfloat16)

time: 255 us -> 289 us (1.13)
  the two profiles are of different devices: /device:TPU:1 before, /device:TPU:2 now
where the time goes in v1:
time: 289 us; the launch traced here: 287 us
  blocking collectives  107 us (37%)
  waiting for transfers between devices  106 us (37%)
  starting transfers between devices  40.4 us (14%)
  between operations  14.1 us (5%)
  matrix products  9.58 us (3%)
  local copies, waits for them, and re-layouts  5.24 us (2%)
  other arithmetic  4.06 us (1%)
    ppermute x15, waiting for transfers between devices, shards(): lax.ppermute(ring[-1], 'kv', [(dev, (dev + 1) % 16) for dev in range(16)])  94.9 us
    psum x1, blocking collectives, shards(): stream_total = lax.psum(jnp.sum(after_wide * after_wide, axis=1), 'kv')  36.7 us
    all_gather x1, blocking collectives, shards(): lax.all_gather(w_mix_out, 'tp', axis=1, tiled=True)  33 us
    ppermute x15, starting transfers between devices, shards(): lax.ppermute(ring[-1], 'kv', [(dev, (dev + 1) % 16) for dev in range(16)])  30.1 us
    all_gather x1, blocking collectives, shards(): hidden_in = lax.all_gather(hidden_own, 'kv', axis=1, tiled=True)  22.4 us
    all_to_all x1, blocking collectives, summed_on_arrival(): lax.all_to_all(split_up(value, dim, devices), axis, 0, 0, tiled=True)  15.1 us
    all_to_all x1, waiting for transfers between devices, summed_on_arrival(): lax.all_to_all(split_up(value, dim, devices), axis, 0, 0, tiled=True)  5.87 us
  transfers between devices with their start and end apart: 20, of which 16 were waited for; matrix products, arithmetic and copies ran while one was open for 4% of the time, Pallas kernels for 0%

profile of v1, /device:TPU:2, one launch (start us, length us, event | category | flops | bytes accessed | tf_op | source)
XLA Modules:
  0.0 286.8 jit_solution(17794049981838269960)
XLA Ops:
  9.6 3.4 %collective-permute-start = (bf16[16,128]{1,0:T(8,128)(2,1)}, bf16[16,128]{1,0:T(8,128)(2,1)S(1)}, u32[]{:S(2)}, u32[]{:S(2)}) collective-permute-start(bf16[16,128]{1,0:T(8,128)(2,1)} %param.15), channel_id=1, source_target_pairs={{0,32},{32,64},{64,96},{96,128},{128,160},{160,192},{192,224},{224... | collective-permute-start | bytes 12296 | tf_op jit(solution)/shard_map/ppermute | solution.py:65
  13.0 6.2 %collective-permute-done = bf16[16,128]{1,0:T(8,128)(2,1)S(1)} collective-permute-done((bf16[16,128]{1,0:T(8,128)(2,1)}, bf16[16,128]{1,0:T(8,128)(2,1)S(1)}, u32[]{:S(2)}, u32[]{:S(2)}) %collective-permute-start) | collective-permute-done | bytes 4128 | tf_op jit(solution)/shard_map/ppermute | solution.py:65
  21.1 6.9 %collective-permute-done.1 = bf16[16,128]{1,0:T(8,128)(2,1)S(1)} collective-permute-done((bf16[16,128]{1,0:T(8,128)(2,1)S(1)}, bf16[16,128]{1,0:T(8,128)(2,1)S(1)}, u32[]{:S(2)}, u32[]{:S(2)}) %collective-permute-start.1) | collective-permute-done | bytes 4128 | tf_op jit(solution)/shard_map/ppermute | solution.py:65
  29.9 6.9 %collective-permute-done.2 = bf16[16,128]{1,0:T(8,128)(2,1)S(1)} collective-permute-done((bf16[16,128]{1,0:T(8,128)(2,1)S(1)}, bf16[16,128]{1,0:T(8,128)(2,1)S(1)}, u32[]{:S(2)}, u32[]{:S(2)}) %collective-permute-start.2) | collective-permute-done | bytes 4128 | tf_op jit(solution)/shard_map/ppermute | solution.py:65
  38.7 6.9 %collective-permute-done.3 = bf16[16,128]{1,0:T(8,128)(2,1)S(1)} collective-permute-done((bf16[16,128]{1,0:T(8,128)(2,1)S(1)}, bf16[16,128]{1,0:T(8,128)(2,1)S(1)}, u32[]{:S(2)}, u32[]{:S(2)}) %collective-permute-start.3) | collective-permute-done | bytes 4128 | tf_op jit(solution)/shard_map/ppermute | solution.py:65
  47.5 6.9 %collective-permute-done.4 = bf16[16,128]{1,0:T(8,128)(2,1)S(1)} collective-permute-done((bf16[16,128]{1,0:T(8,128)(2,1)S(1)}, bf16[16,128]{1,0:T(8,128)(2,1)S(1)}, u32[]{:S(2)}, u32[]{:S(2)}) %collective-permute-start.4) | collective-permute-done | bytes 4128 | tf_op jit(solution)/shard_map/ppermute | solution.py:65
  56.3 6.9 %collective-permute-done.5 = bf16[16,128]{1,0:T(8,128)(2,1)S(1)} collective-permute-done((bf16[16,128]{1,0:T(8,128)(2,1)S(1)}, bf16[16,128]{1,0:T(8,128)(2,1)S(1)}, u32[]{:S(2)}, u32[]{:S(2)}) %collective-permute-start.5) | collective-permute-done | bytes 4128 | tf_op jit(solution)/shard_map/ppermute | solution.py:65
  65.1 6.9 %collective-permute-done.6 = bf16[16,128]{1,0:T(8,128)(2,1)S(1)} collective-permute-done((bf16[16,128]{1,0:T(8,128)(2,1)S(1)}, bf16[16,128]{1,0:T(8,128)(2,1)S(1)}, u32[]{:S(2)}, u32[]{:S(2)}) %collective-permute-start.6) | collective-permute-done | bytes 4128 | tf_op jit(solution)/shard_map/ppermute | solution.py:65
  73.9 6.9 %collective-permute-done.7 = bf16[16,128]{1,0:T(8,128)(2,1)S(1)} collective-permute-done((bf16[16,128]{1,0:T(8,128)(2,1)S(1)}, bf16[16,128]{1,0:T(8,128)(2,1)S(1)}, u32[]{:S(2)}, u32[]{:S(2)}) %collective-permute-start.7) | collective-permute-done | bytes 4128 | tf_op jit(solution)/shard_map/ppermute | solution.py:65
  82.7 6.9 %collective-permute-done.8 = bf16[16,128]{1,0:T(8,128)(2,1)S(1)} collective-permute-done((bf16[16,128]{1,0:T(8,128)(2,1)S(1)}, bf16[16,128]{1,0:T(8,128)(2,1)S(1)}, u32[]{:S(2)}, u32[]{:S(2)}) %collective-permute-start.8) | collective-permute-done | bytes 4128 | tf_op jit(solution)/shard_map/ppermute | solution.py:65
  91.5 6.9 %collective-permute-done.9 = bf16[16,128]{1,0:T(8,128)(2,1)S(1)} collective-permute-done((bf16[16,128]{1,0:T(8,128)(2,1)S(1)}, bf16[16,128]{1,0:T(8,128)(2,1)S(1)}, u32[]{:S(2)}, u32[]{:S(2)}) %collective-permute-start.9) | collective-permute-done | bytes 4128 | tf_op jit(solution)/shard_map/ppermute | solution.py:65
  100.3 6.9 %collective-permute-done.10 = bf16[16,128]{1,0:T(8,128)(2,1)S(1)} collective-permute-done((bf16[16,128]{1,0:T(8,128)(2,1)S(1)}, bf16[16,128]{1,0:T(8,128)(2,1)S(1)}, u32[]{:S(2)}, u32[]{:S(2)}) %collective-permute-start.10) | collective-permute-done | bytes 4128 | tf_op jit(solution)/shard_map/ppermute | solution.py:65
  109.2 6.9 %collective-permute-done.11 = bf16[16,128]{1,0:T(8,128)(2,1)S(1)} collective-permute-done((bf16[16,128]{1,0:T(8,128)(2,1)S(1)}, bf16[16,128]{1,0:T(8,128)(2,1)S(1)}, u32[]{:S(2)}, u32[]{:S(2)}) %collective-permute-start.11) | collective-permute-done | bytes 4128 | tf_op jit(solution)/shard_map/ppermute | solution.py:65
  118.0 6.9 %collective-permute-done.12 = bf16[16,128]{1,0:T(8,128)(2,1)S(1)} collective-permute-done((bf16[16,128]{1,0:T(8,128)(2,1)S(1)}, bf16[16,128]{1,0:T(8,128)(2,1)S(1)}, u32[]{:S(2)}, u32[]{:S(2)}) %collective-permute-start.12) | collective-permute-done | bytes 4128 | tf_op jit(solution)/shard_map/ppermute | solution.py:65
  126.8 33.0 %all_gather.16 = bf16[128,2048]{0,1:T(8,128)(2,1)S(1)} all-gather(bf16[128,64]{0,1:T(8,128)(2,1)} %param.23), channel_id=1, replica_groups=mesh['kv'=16,'tp'=32] {'tp'}, dimensions={1}, use_global_device_ids=true | all-gather | bytes 540672 | tf_op jit(solution)/shard_map/all_gather | solution.py:102
  162.3 6.0 %collective-permute-done.14 = bf16[16,128]{1,0:T(8,128)(2,1)S(1)} collective-permute-done((bf16[16,128]{1,0:T(8,128)(2,1)S(1)}, bf16[16,128]{1,0:T(8,128)(2,1)S(1)}, u32[]{:S(2)}, u32[]{:S(2)}) %collective-permute-start.14) | collective-permute-done | bytes 4128 | tf_op jit(solution)/shard_map/ppermute | solution.py:65
  177.4 15.1 %all_to_all.16 = f32[16,16,128]{2,1,0:T(8,128)S(1)} all-to-all(f32[16,16,128]{2,1,0:T(8,128)S(1)} %convolution_bitcast_fusion), channel_id=1, replica_groups=mesh['kv'=16,'tp'=32] {'kv'}, dimensions={0} | all-to-all | bytes 262144 | tf_op jit(solution)/shard_map/all_to_all | solution.py:24
  193.3 4.7 %all-to-all-start.1 = ((f32[16,1,16]{2,1,0:T(1,128)}), f32[16,1,16]{2,1,0:T(1,128)S(1)}, u32[]{:S(2)}, u32[]{:S(2)}) async-start(f32[16,1,16]{2,1,0:T(1,128)} %broadcast_in_dim.2), calls=%async_computation.1 | async-start | bytes 16384 | tf_op jit(solution)/shard_map/all_to_all | solution.py:30
  199.5 4.8 %all-to-all-done.1 = f32[16,1,16]{2,1,0:T(1,128)S(1)} async-done(((f32[16,1,16]{2,1,0:T(1,128)}), f32[16,1,16]{2,1,0:T(1,128)S(1)}, u32[]{:S(2)}, u32[]{:S(2)}) %all-to-all-start.1) | async-done | bytes 1056 | tf_op jit(solution)/shard_map/all_to_all | solution.py:30
  204.5 36.7 %psum.7 = f32[16]{0:T(128)S(1)} all-reduce(f32[16]{0:T(128)S(1)} %get-tuple-element.2), channel_id=1, replica_groups=mesh['kv'=16,'tp'=32] {'kv'}, use_global_device_ids=true, to_apply=%region_6.7 | all-reduce | flops 16 | bytes 128 | tf_op jit(solution)/shard_map/psum | solution.py:113
  241.3 22.4 %all_gather.17 = bf16[16,2048]{1,0:T(8,128)(2,1)S(1)} all-gather(bf16[16,128]{1,0:T(8,128)(2,1)S(1)} %fusion.32), channel_id=1, replica_groups=mesh['kv'=16,'tp'=32] {'kv'}, dimensions={1}, use_global_device_ids=true | all-gather | bytes 69632 | tf_op jit(solution)/shard_map/all_gather | solution.py:117
  263.7 3.2 %convolution_bitcast_fusion.1 = f32[2,16,8,128]{3,2,1,0:T(8,128)S(1)} fusion(bf16[512,2048]{0,1:T(8,128)(2,1)} %all-gather.8.cloned.1.call-done, bf16[16,2048]{1,0:T(8,128)(2,1)S(1)} %all_gather.17, bf16[2048,512]{1,0:T(8,128)(2,1)} %all-gather.6.cloned.1.call-done), kind=kOutput, calls=%fused_computation.1 | convolution fusion | flops 67133440 | bytes 4390912 | tf_op jit(solution)/shard_map/dot_general | solution.py:125
  267.6 5.4 %all-to-all-start.2 = ((f32[16,16,128]{2,1,0:T(8,128)}), f32[16,16,128]{2,1,0:T(8,128)S(1)}, u32[]{:S(2)}, u32[]{:S(2)}) async-start(f32[16,16,128]{2,1,0:T(8,128)} %bitcast.30), calls=%async_computation.2 | async-start | bytes 262144 | tf_op jit(solution)/shard_map/all_to_all | solution.py:24
  273.8 5.9 %all-to-all-done.2 = f32[16,16,128]{2,1,0:T(8,128)S(1)} async-done(((f32[16,16,128]{2,1,0:T(8,128)}), f32[16,16,128]{2,1,0:T(8,128)S(1)}, u32[]{:S(2)}, u32[]{:S(2)}) %all-to-all-start.2) | async-done | bytes 131104 | tf_op jit(solution)/shard_map/all_to_all | solution.py:24
  (94 shorter events, 43.3 us)
Async XLA Ops:
  7.2 165.7 %copy-start.5 = (f32[128]{0:T(128)S(1)}, f32[128]{0:T(128)}, u32[]{:S(2)}) copy-start(f32[128]{0:T(128)} %param.21) | copy-start | bytes 1540
  7.2 165.7 %copy-start.3 = (f32[2048]{0:T(1024)S(1)}, f32[2048]{0:T(1024)}, u32[]{:S(2)}) copy-start(f32[2048]{0:T(1024)} %param.24) | copy-start | bytes 24580
  7.2 167.0 %copy-start.1 = (f32[16,1,128,128]{3,2,1,0:T(8,128)S(1)}, f32[16,1,128,128]{3,2,1,0:T(8,128)}, u32[]{:S(2)}) copy-start(f32[16,1,128,128]{3,2,1,0:T(8,128)} %param.16) | copy-start | bytes 3145732
  7.2 163.0 %all-gather.4.cloned.1.call-start = ((), (), s32[]{:S(2)}) async-start(), calls=%async_computation.3 | async-start | bytes 2162688 | tf_op jit(solution)/shard_map/all_gather | solution.py:13
  8.8 255.0 %all-gather.6.cloned.1.call-start = ((), (), s32[]{:S(2)}) async-start(), calls=%async_computation.4 | async-start | bytes 2162688 | tf_op jit(solution)/shard_map/all_gather | solution.py:121
  9.5 254.2 %all-gather.8.cloned.1.call-start = ((), (), s32[]{:S(2)}) async-start(), calls=%async_computation.5 | async-start | bytes 2162688 | tf_op jit(solution)/shard_map/all_gather | solution.py:127
  9.6 9.6 %collective-permute-start = (bf16[16,128]{1,0:T(8,128)(2,1)}, bf16[16,128]{1,0:T(8,128)(2,1)S(1)}, u32[]{:S(2)}, u32[]{:S(2)}) collective-permute-start(bf16[16,128]{1,0:T(8,128)(2,1)} %param.15), channel_id=1, source_target_pairs={{0,32},{32,64},{64,96},{96,128},{128,160},{160,192},{192,224},{224... | collective-permute-start | bytes 12296 | tf_op jit(solution)/shard_map/ppermute | solution.py:65
  19.1 8.8 %collective-permute-start.1 = (bf16[16,128]{1,0:T(8,128)(2,1)S(1)}, bf16[16,128]{1,0:T(8,128)(2,1)S(1)}, u32[]{:S(2)}, u32[]{:S(2)}) collective-permute-start(bf16[16,128]{1,0:T(8,128)(2,1)S(1)} %collective-permute-done), channel_id=1, source_target_pairs={{0,32},{32,64},{64,96},{96,128},{128,160},{160,192},{192,224},{224... | collective-permute-start | bytes 12296 | tf_op jit(solution)/shard_map/ppermute | solution.py:65
  27.9 8.8 %collective-permute-start.2 = (bf16[16,128]{1,0:T(8,128)(2,1)S(1)}, bf16[16,128]{1,0:T(8,128)(2,1)S(1)}, u32[]{:S(2)}, u32[]{:S(2)}) collective-permute-start(bf16[16,128]{1,0:T(8,128)(2,1)S(1)} %collective-permute-done.1), channel_id=1, source_target_pairs={{0,32},{32,64},{64,96},{96,128},{128,160},{160,192},{192,224},{224... | collective-permute-start | bytes 12296 | tf_op jit(solution)/shard_map/ppermute | solution.py:65
  36.8 8.8 %collective-permute-start.3 = (bf16[16,128]{1,0:T(8,128)(2,1)S(1)}, bf16[16,128]{1,0:T(8,128)(2,1)S(1)}, u32[]{:S(2)}, u32[]{:S(2)}) collective-permute-start(bf16[16,128]{1,0:T(8,128)(2,1)S(1)} %collective-permute-done.2), channel_id=1, source_target_pairs={{0,32},{32,64},{64,96},{96,128},{128,160},{160,192},{192,224},{224... | collective-permute-start | bytes 12296 | tf_op jit(solution)/shard_map/ppermute | solution.py:65
  45.6 8.8 %collective-permute-start.4 = (bf16[16,128]{1,0:T(8,128)(2,1)S(1)}, bf16[16,128]{1,0:T(8,128)(2,1)S(1)}, u32[]{:S(2)}, u32[]{:S(2)}) collective-permute-start(bf16[16,128]{1,0:T(8,128)(2,1)S(1)} %collective-permute-done.3), channel_id=1, source_target_pairs={{0,32},{32,64},{64,96},{96,128},{128,160},{160,192},{192,224},{224... | collective-permute-start | bytes 12296 | tf_op jit(solution)/shard_map/ppermute | solution.py:65
  54.4 8.8 %collective-permute-start.5 = (bf16[16,128]{1,0:T(8,128)(2,1)S(1)}, bf16[16,128]{1,0:T(8,128)(2,1)S(1)}, u32[]{:S(2)}, u32[]{:S(2)}) collective-permute-start(bf16[16,128]{1,0:T(8,128)(2,1)S(1)} %collective-permute-done.4), channel_id=1, source_target_pairs={{0,32},{32,64},{64,96},{96,128},{128,160},{160,192},{192,224},{224... | collective-permute-start | bytes 12296 | tf_op jit(solution)/shard_map/ppermute | solution.py:65
  63.2 8.8 %collective-permute-start.6 = (bf16[16,128]{1,0:T(8,128)(2,1)S(1)}, bf16[16,128]{1,0:T(8,128)(2,1)S(1)}, u32[]{:S(2)}, u32[]{:S(2)}) collective-permute-start(bf16[16,128]{1,0:T(8,128)(2,1)S(1)} %collective-permute-done.5), channel_id=1, source_target_pairs={{0,32},{32,64},{64,96},{96,128},{128,160},{160,192},{192,224},{224... | collective-permute-start | bytes 12296 | tf_op jit(solution)/shard_map/ppermute | solution.py:65
  72.0 8.8 %collective-permute-start.7 = (bf16[16,128]{1,0:T(8,128)(2,1)S(1)}, bf16[16,128]{1,0:T(8,128)(2,1)S(1)}, u32[]{:S(2)}, u32[]{:S(2)}) collective-permute-start(bf16[16,128]{1,0:T(8,128)(2,1)S(1)} %collective-permute-done.6), channel_id=1, source_target_pairs={{0,32},{32,64},{64,96},{96,128},{128,160},{160,192},{192,224},{224... | collective-permute-start | bytes 12296 | tf_op jit(solution)/shard_map/ppermute | solution.py:65
  80.8 8.8 %collective-permute-start.8 = (bf16[16,128]{1,0:T(8,128)(2,1)S(1)}, bf16[16,128]{1,0:T(8,128)(2,1)S(1)}, u32[]{:S(2)}, u32[]{:S(2)}) collective-permute-start(bf16[16,128]{1,0:T(8,128)(2,1)S(1)} %collective-permute-done.7), channel_id=1, source_target_pairs={{0,32},{32,64},{64,96},{96,128},{128,160},{160,192},{192,224},{224... | collective-permute-start | bytes 12296 | tf_op jit(solution)/shard_map/ppermute | solution.py:65
  89.6 8.8 %collective-permute-start.9 = (bf16[16,128]{1,0:T(8,128)(2,1)S(1)}, bf16[16,128]{1,0:T(8,128)(2,1)S(1)}, u32[]{:S(2)}, u32[]{:S(2)}) collective-permute-start(bf16[16,128]{1,0:T(8,128)(2,1)S(1)} %collective-permute-done.8), channel_id=1, source_target_pairs={{0,32},{32,64},{64,96},{96,128},{128,160},{160,192},{192,224},{224... | collective-permute-start | bytes 12296 | tf_op jit(solution)/shard_map/ppermute | solution.py:65
  98.4 8.8 %collective-permute-start.10 = (bf16[16,128]{1,0:T(8,128)(2,1)S(1)}, bf16[16,128]{1,0:T(8,128)(2,1)S(1)}, u32[]{:S(2)}, u32[]{:S(2)}) collective-permute-start(bf16[16,128]{1,0:T(8,128)(2,1)S(1)} %collective-permute-done.9), channel_id=1, source_target_pairs={{0,32},{32,64},{64,96},{96,128},{128,160},{160,192},{192,224},{224... | collective-permute-start | bytes 12296 | tf_op jit(solution)/shard_map/ppermute | solution.py:65
  107.2 8.8 %collective-permute-start.11 = (bf16[16,128]{1,0:T(8,128)(2,1)S(1)}, bf16[16,128]{1,0:T(8,128)(2,1)S(1)}, u32[]{:S(2)}, u32[]{:S(2)}) collective-permute-start(bf16[16,128]{1,0:T(8,128)(2,1)S(1)} %collective-permute-done.10), channel_id=1, source_target_pairs={{0,32},{32,64},{64,96},{96,128},{128,160},{160,192},{192,224},{224... | collective-permute-start | bytes 12296 | tf_op jit(solution)/shard_map/ppermute | solution.py:65
  116.0 8.8 %collective-permute-start.12 = (bf16[16,128]{1,0:T(8,128)(2,1)S(1)}, bf16[16,128]{1,0:T(8,128)(2,1)S(1)}, u32[]{:S(2)}, u32[]{:S(2)}) collective-permute-start(bf16[16,128]{1,0:T(8,128)(2,1)S(1)} %collective-permute-done.11), channel_id=1, source_target_pairs={{0,32},{32,64},{64,96},{96,128},{128,160},{160,192},{192,224},{224... | collective-permute-start | bytes 12296 | tf_op jit(solution)/shard_map/ppermute | solution.py:65
  124.9 34.9 %collective-permute-start.13 = (bf16[16,128]{1,0:T(8,128)(2,1)S(1)}, bf16[16,128]{1,0:T(8,128)(2,1)S(1)}, u32[]{:S(2)}, u32[]{:S(2)}) collective-permute-start(bf16[16,128]{1,0:T(8,128)(2,1)S(1)} %collective-permute-done.12), channel_id=1, source_target_pairs={{0,32},{32,64},{64,96},{96,128},{128,160},{160,192},{192,224},{224... | collective-permute-start | bytes 12296 | tf_op jit(solution)/shard_map/ppermute | solution.py:65
  159.7 8.6 %collective-permute-start.14 = (bf16[16,128]{1,0:T(8,128)(2,1)S(1)}, bf16[16,128]{1,0:T(8,128)(2,1)S(1)}, u32[]{:S(2)}, u32[]{:S(2)}) collective-permute-start(bf16[16,128]{1,0:T(8,128)(2,1)S(1)} %collective-permute-done.13), channel_id=1, source_target_pairs={{0,32},{32,64},{64,96},{96,128},{128,160},{160,192},{192,224},{224... | collective-permute-start | bytes 12296 | tf_op jit(solution)/shard_map/ppermute | solution.py:65
  174.8 92.1 %copy-start = (f32[16,1,128,128]{3,2,1,0:T(8,128)}, f32[16,1,128,128]{3,2,1,0:T(8,128)S(1)}, u32[]{:S(2)}) copy-start(f32[16,1,128,128]{3,2,1,0:T(8,128)S(1)} %multiply_add_fusion) | copy-start | bytes 3145732
  193.3 11.0 %all-to-all-start.1 = ((f32[16,1,16]{2,1,0:T(1,128)}), f32[16,1,16]{2,1,0:T(1,128)S(1)}, u32[]{:S(2)}, u32[]{:S(2)}) async-start(f32[16,1,16]{2,1,0:T(1,128)} %broadcast_in_dim.2), calls=%async_computation.1 | async-start | bytes 16384 | tf_op jit(solution)/shard_map/all_to_all | solution.py:30
  267.6 12.0 %all-to-all-start.2 = ((f32[16,16,128]{2,1,0:T(8,128)}), f32[16,16,128]{2,1,0:T(8,128)S(1)}, u32[]{:S(2)}, u32[]{:S(2)}) async-start(f32[16,16,128]{2,1,0:T(8,128)} %bitcast.30), calls=%async_computation.2 | async-start | bytes 262144 | tf_op jit(solution)/shard_map/all_to_all | solution.py:24
  (2 other events, 33.2 us)
Sparse Core Ops, SparseCore 0:
  10.7 75.8 all-gather.3
  88.7 68.6 all-gather.5
  159.6 68.3 all-gather.7
